TPU v7x, 512 devices: a whole 4x8x8 slice. The times are simulated.
512 devices in a mesh: sp: 64 (over z, y), tp: 8 (over x, core).
Axes of the slice: x: 4, y: 8, z: 8, core: 2. Of those that a mesh axis runs over, the one named last changes fastest.
Arguments:
- resid: bfloat16 [32768, 2048], P('sp'), may hold values from -6 to 6
- queries: bfloat16 [32768, 2048], P('sp', 'tp'), may hold values from -6 to 6
- keys: bfloat16 [32768, 512], P('sp', 'tp'), may hold values from -6 to 6
- values: bfloat16 [32768, 512], P('sp', 'tp'), may hold values from -6 to 6
- documents: int32 [32768], P('sp'), may hold values from 0 to 31, never falling along the last dimension, each value on 1 to 2048 neighbouring positions
- q_gain: float32 [64], replicated, may hold values from 0.5 to 6.5
- k_gain: float32 [64], replicated, may hold values from 0.5 to 6.5
- sink: float32 [32], P('tp'), may hold values from -1 to 5
- w_out: bfloat16 [2048, 2048], P('tp'), may hold values from -0.5 to 0.5
- n_gain: float32 [2048], replicated, may hold values from 0.1 to 1.9
- w_up: bfloat16 [2048, 8192], P('sp', 'tp'), may hold values from -0.125 to 0.125
- w_down: bfloat16 [8192, 2048], P('tp', 'sp'), may hold values from -0.0625 to 0.0625
Outputs:
- layer_out: bfloat16 [32768, 2048], P('sp')
All inputs are finite; a program needn't handle non-finite values.
Results may differ from a plain program's by a relative error of at most 0.018.
The roundings to bfloat16 on the way count: a program that leaves them out, or rounds other values in their place, can miss the bound.
Values may be sent and summed in bfloat16 or wider, within the bound.
A program may use at most 64 MiB of HBM per device.

v0:
```python
import jax
import jax.numpy as jnp
from jax import lax
from jax.sharding import PartitionSpec as P

WINDOW = 128
EPS = 1e-06


def gather_turned(arrays, axis, dims):
    turned = [jnp.moveaxis(a, dim, 0) for a, dim in zip(arrays, dims)]
    both = jnp.concatenate([t.reshape(len(t), -1) for t in turned], axis=1)
    result, at, outs = (lax.all_gather(both, axis, axis=0, tiled=True), 0, [])
    for t, dim in zip(turned, dims):
        section = result[:, at : at + t[0].size].reshape(-1, *t.shape[1:])
        outs.append(jnp.moveaxis(section, 0, dim))
        at += t[0].size
    return tuple(outs)


def extended(x, sides, width):
    for axis, dim in sides:
        count, length = (lax.axis_size(axis), x.shape[dim])
        up = [(i, (i + 1) % count) for i in range(count - 1)]
        down = [(j, i) for i, j in up]
        last = lax.slice_in_dim(x, length - width, length, axis=dim)
        initial = lax.slice_in_dim(x, 0, width, axis=dim)
        before = lax.ppermute(last, axis, up)
        after = lax.ppermute(initial, axis, down)
        x = jnp.concatenate([before, x, after], axis=dim)
    return x


def in_blocks(x, dim, count):
    dims = x.shape
    tiles = x.reshape(*dims[:dim], count, dims[dim] // count, *dims[dim + 1 :])
    return jnp.moveaxis(tiles, dim, 0)


def summed_on_arrival(x, axis, dim):
    count = lax.axis_size(axis)
    tiles = lax.all_to_all(in_blocks(x, dim, count), axis, 0, 0, tiled=True)
    return jnp.sum(tiles.astype(jnp.float32), axis=0)


def joined_along(tiles, dim):
    dims = list(tiles.shape[1:])
    dims[dim] *= tiles.shape[0]
    return jnp.moveaxis(tiles, 0, dim).reshape(dims)


def copy_for_each(x, axis):
    copies = jnp.broadcast_to(x, (lax.axis_size(axis), *x.shape))
    return lax.all_to_all(copies, axis, split_axis=0, concat_axis=0, tiled=True)


def collect(x, axis, dim):
    return joined_along(copy_for_each(x, axis), dim)


def rms_scale(field, gain):
    wide = field.astype(jnp.float32)
    return wide * lax.rsqrt(jnp.mean(wide * wide, axis=-1, keepdims=True) + EPS) * gain


def mixer_partial(normed, gathered):
    upward = jnp.dot(normed, gathered[0], preferred_element_type=jnp.float32)
    active = jnp.square(jax.nn.relu(upward)).astype(jnp.bfloat16)
    return jnp.dot(active, gathered[1], preferred_element_type=jnp.float32)


def shards(
    resid, queries, keys, values, documents, q_gain, k_gain, sink, w_out, n_gain, w_up, w_down
):
    rows = resid.shape[0]
    head_size = q_gain.shape[0]
    heads_here = sink.shape[0]
    kv_here = keys.shape[1] // head_size
    group = heads_here // kv_here
    gathered = None
    gathered = gather_turned((w_up, w_down), "sp", (0, 1))
    qnorm = rms_scale(queries.reshape(rows, kv_here, group, head_size), q_gain).astype(jnp.bfloat16)
    knorm = rms_scale(keys.reshape(rows, kv_here, head_size), k_gain).astype(jnp.bfloat16)
    vheads = values.reshape(rows, kv_here, head_size)
    doc_here = documents.astype(jnp.bfloat16)
    near_keys, near_values, near_docs = (
        extended(knorm, (("sp", 0),), WINDOW),
        extended(vheads, (("sp", 0),), WINDOW),
        extended(doc_here, (("sp", 0),), WINDOW),
    )
    offset = lax.axis_index("sp") * rows
    total = rows * lax.axis_size("sp")
    query_pos = offset + jnp.arange(rows, dtype=jnp.int32)
    key_pos = offset - WINDOW + jnp.arange(rows + 2 * WINDOW, dtype=jnp.int32)
    distance = key_pos[None, :] - query_pos[:, None]
    allowed = (jnp.abs(distance) <= WINDOW) & (key_pos[None, :] >= 0) & (key_pos[None, :] < total)
    allowed = allowed & (near_docs[None, :] == doc_here[:, None])
    heads_all = heads_here * lax.axis_size("tp")
    first_head = (lax.axis_index("tp") * heads_here).astype(jnp.float32)
    slopes = jnp.exp2(
        -8.0 * (first_head + jnp.arange(heads_here, dtype=jnp.float32) + 1.0) / heads_all
    )
    slopes = slopes.reshape(kv_here, group)
    sink_f = sink.reshape(kv_here, group)
    scores = jnp.einsum(
        "rkgd,skd->kgrs", qnorm, near_keys, preferred_element_type=jnp.float32
    ) * head_size ** (-0.5)
    scores = scores - slopes[:, :, None, None] * jnp.abs(distance).astype(jnp.float32)[None, None]
    scores = jnp.where(allowed[None, None], scores, jnp.float32(-1e30))
    highest = jnp.maximum(jnp.max(scores, axis=-1), sink_f[:, :, None])
    weights = jnp.exp(scores - highest[..., None])
    denom = jnp.sum(weights, axis=-1) + jnp.exp(sink_f[:, :, None] - highest)
    summed = jnp.einsum(
        "kgrs,skd->rkgd",
        weights.astype(jnp.bfloat16),
        near_values,
        preferred_element_type=jnp.float32,
    )
    attended = (
        (summed / denom.transpose(2, 0, 1)[..., None])
        .astype(jnp.bfloat16)
        .reshape(rows, heads_here * head_size)
    )
    share = rows // lax.axis_size("tp")
    head_mix = summed_on_arrival(
        jnp.dot(attended, w_out, preferred_element_type=jnp.float32).astype(jnp.bfloat16), "tp", 0
    )
    own_resid = lax.dynamic_slice_in_dim(resid, lax.axis_index("tp") * share, share, 0)
    middle = (own_resid.astype(jnp.float32) + head_mix).astype(jnp.bfloat16)
    normed_part = rms_scale(middle, n_gain).astype(jnp.bfloat16)
    normed = collect(normed_part, "tp", 0)
    partial_sum = mixer_partial(normed, gathered)
    unit_mix = summed_on_arrival(partial_sum.astype(jnp.bfloat16), "tp", 0)
    finished = (middle.astype(jnp.float32) + unit_mix).astype(jnp.bfloat16)
    return collect(finished, "tp", 0)


def solution(mesh):
    placed = (
        P("sp", None),
        P("sp", "tp"),
        P("sp", "tp"),
        P("sp", "tp"),
        P("sp"),
        P(),
        P(),
        P("tp"),
        P("tp", None),
        P(),
        P("sp", "tp"),
        P("tp", "sp"),
    )
    return jax.shard_map(
        shards, mesh=mesh, in_specs=placed, out_specs=P("sp", None), check_vma=False
    )
```

profile of v0, /device:TPU:1, one launch (start us, length us, event | category | flops | bytes accessed | tf_op | source)
XLA Modules:
  0.0 194.1 jit_solution(1907560911907022125)
XLA Ops:
  6.5 1.6 pad_maximum_fusion
  8.2 0.0 all-gather.2.cloned.1.call-update
  8.2 0.7 convert_element_type.85
  8.9 4.0 %collective-permute-start.2 = (bf16[128]{0:T(256)(128)(2,1)S(1)}, bf16[128]{0:T(256)(128)(2,1)S(1)}, u32[]{:S(2)}, u32[]{:S(2)}) collective-permute-start(bf16[128]{0:T(256)(128)(2,1)S(1)} %get-tuple-element.11), channel_id=1, source_target_pairs={{0,8},{8,16},{16,24},{24,32},{32,40},{40,48},{48,56},{56,64},{64,7... | collective-permute-start | bytes 776 | tf_op jit(solution)/shard_map/ppermute | solution.py:28
  12.9 1.3 collective-permute-start.3
  14.2 0.9 fusion.39
  15.1 0.9 fusion.41
  16.0 4.0 %collective-permute-start.4 = (bf16[128,1,64]{0,2,1:T(8,128)(2,1)S(1)}, bf16[128,1,64]{0,2,1:T(8,128)(2,1)S(1)}, u32[]{:S(2)}, u32[]{:S(2)}) collective-permute-start(bf16[128,1,64]{0,2,1:T(8,128)(2,1)S(1)} %get-tuple-element.9), channel_id=1, source_target_pairs={{0,8},{8,16},{16,24},{24,32},{32,40},{40,48},{48,56},{56,64},{64,7... | collective-permute-start | bytes 49160 | tf_op jit(solution)/shard_map/ppermute | solution.py:28
  20.0 1.3 collective-permute-start.5
  21.3 0.7 slice_bitcast_fusion.3
  22.1 4.0 %collective-permute-start = (bf16[128,1,64]{0,2,1:T(8,128)(2,1)S(1)}, bf16[128,1,64]{0,2,1:T(8,128)(2,1)S(1)}, u32[]{:S(2)}, u32[]{:S(2)}) collective-permute-start(bf16[128,1,64]{0,2,1:T(8,128)(2,1)S(1)} %get-tuple-element.7), channel_id=1, source_target_pairs={{0,8},{8,16},{16,24},{24,32},{32,40},{40,48},{48,56},{56,64},{64,7... | collective-permute-start | bytes 49160 | tf_op jit(solution)/shard_map/ppermute | solution.py:28
  26.1 1.1 copy.15
  27.2 0.1 bitcast_reduce_fusion
  27.3 0.9 fusion.67
  28.2 0.3 fusion.16
  28.6 0.7 mul.141
  29.2 0.1 mul.142
  29.3 0.1 fusion.34
  29.4 0.0 collective-permute-done.2
  29.4 1.3 collective-permute-start.1
  30.8 0.0 collective-permute-done.3
  30.8 1.0 fusion.20
  31.8 0.0 collective-permute-done.4
  31.8 0.0 copy-start.3
  31.8 1.9 fusion.7
  33.7 0.0 copy-start.1
  33.7 0.1 broadcast_maximum_fusion
  33.8 1.9 fusion.1
  35.6 0.1 fusion.54
  35.7 0.0 collective-permute-done
  35.7 0.0 collective-permute-done.1
  35.8 2.3 %fusion.30 = bf16[512,1,4,64]{0,3,2,1:T(8,128)(2,1)S(1)} fusion(f32[768,512,4]{1,0,2:T(8,128)S(1)} %get-tuple-element.14, f32[4,512]{1,0:T(4,128)S(1)} %broadcast_maximum_fusion, f32[512,768]{0,1:T(8,128)S(1)} %fusion.16, f32[4]{0:T(128)S(1)} %multiply_exponential_fusion, pred[512,768]{0,1:T(8,128)(4,1)S(1)} %fusion.20, f32[512,4]{0,1:T(4,128)S(1)} %fusion.54, ...), kind=kOutput, calls=%fused_computation.26 | convolution fusion | flops 211320832 | bytes 8634384 | tf_op jit(solution)/shard_map/kgrs,skd->rkgd/dot_general | solution.py:113
  38.1 2.1 %convolution_convert_fusion = bf16[512,2048]{1,0:T(8,128)(2,1)} fusion(bf16[512,256]{0,1:T(8,128)(2,1)S(1)} %bitcast.93, bf16[256,2048]{1,0:T(8,128)(2,1)S(1)} %copy-done), kind=kOutput, calls=%fused_computation.15 | convolution fusion | flops 537919488 | bytes 3407872 | tf_op jit(solution)/shard_map/dot_general | solution.py:126
  40.2 8.9 %all-to-all-start = ((bf16[8,64,2048]{2,1,0:T(8,128)(2,1)}), bf16[8,64,2048]{2,1,0:T(8,128)(2,1)S(1)}, u32[]{:S(2)}, u32[]{:S(2)}) async-start(bf16[8,64,2048]{2,1,0:T(8,128)(2,1)} %bitcast.23), calls=%async_computation | async-start | bytes 4194304 | tf_op jit(solution)/shard_map/all_to_all | solution.py:42
  49.0 26.2 %all-to-all-done = bf16[8,64,2048]{2,1,0:T(8,128)(2,1)S(1)} async-done(((bf16[8,64,2048]{2,1,0:T(8,128)(2,1)}), bf16[8,64,2048]{2,1,0:T(8,128)(2,1)S(1)}, u32[]{:S(2)}, u32[]{:S(2)}) %all-to-all-start) | async-done | bytes 2097184 | tf_op jit(solution)/shard_map/all_to_all | solution.py:42
  75.3 0.4 convert_reduce_fusion.1
  75.6 1.1 fusion.35
  76.8 0.1 fusion.37
  77.0 0.2 broadcast_in_dim.14
  77.2 29.6 %all_to_all.20 = bf16[8,64,2048]{2,1,0:T(8,128)(2,1)S(1)} all-to-all(bf16[8,64,2048]{2,1,0:T(8,128)(2,1)S(1)} %broadcast_in_dim.14), channel_id=1, replica_groups=mesh['sp'=64,'tp'=8] {'tp'}, dimensions={0} | all-to-all | bytes 4194304 | tf_op jit(solution)/shard_map/all_to_all | solution.py:54
  106.8 8.1 %all-gather.2.cloned.1.call-done = bf16[2048,2048]{1,0:T(8,128)(2,1)} async-done(((bf16[32,2048]{1,0:T(8,128)(2,1)}), bf16[2048,2048]{1,0:T(8,128)(2,1)}) %all-gather.2.cloned.1.call-update) | async-done | bytes 8388624 | tf_op jit(solution)/shard_map/all_gather | solution.py:13
  115.0 9.3 %fusion.11 = bf16[512,2048]{1,0:T(8,128)(2,1)} fusion(bf16[2048,2048]{1,0:T(8,128)(2,1)} %all-gather.2.cloned.1.call-done, bf16[512,2048]{1,0:T(8,128)(2,1)S(1)} %bitcast.91), kind=kOutput, calls=%fused_computation.14 | convolution fusion | flops 4297588736 | bytes 12582912 | tf_op jit(solution)/shard_map/dot_general | solution.py:69
  124.3 31.3 %all_to_all.21 = bf16[8,64,2048]{2,1,0:T(8,128)(2,1)S(1)} all-to-all(bf16[8,64,2048]{2,1,0:T(8,128)(2,1)} %bitcast.92), channel_id=1, replica_groups=mesh['sp'=64,'tp'=8] {'tp'}, dimensions={0} | all-to-all | bytes 4194304 | tf_op jit(solution)/shard_map/all_to_all | solution.py:42
  155.6 0.4 convert_reduce_fusion
  156.0 0.1 fusion.38
  156.1 0.2 broadcast_in_dim.15
  156.3 29.7 %all_to_all.22 = bf16[8,64,2048]{2,1,0:T(8,128)(2,1)S(1)} all-to-all(bf16[8,64,2048]{2,1,0:T(8,128)(2,1)S(1)} %broadcast_in_dim.15), channel_id=1, replica_groups=mesh['sp'=64,'tp'=8] {'tp'}, dimensions={0} | all-to-all | bytes 4194304 | tf_op jit(solution)/shard_map/all_to_all | solution.py:54
  186.0 1.3 copy.19
  (18 shorter events, 0.1 us)
Async XLA Ops:
  6.5 31.6 %copy-start = (bf16[256,2048]{1,0:T(8,128)(2,1)S(1)}, bf16[256,2048]{1,0:T(8,128)(2,1)}, u32[]{:S(2)}) copy-start(bf16[256,2048]{1,0:T(8,128)(2,1)} %param.20) | copy-start | bytes 3145732
  6.5 108.4 %all-gather.2.cloned.1.call-start = ((), (), s32[]{:S(2)}) async-start(), calls=%async_computation.4 | async-start | bytes 8519680 | tf_op jit(solution)/shard_map/all_gather | solution.py:13
  8.9 20.5 %collective-permute-start.2 = (bf16[128]{0:T(256)(128)(2,1)S(1)}, bf16[128]{0:T(256)(128)(2,1)S(1)}, u32[]{:S(2)}, u32[]{:S(2)}) collective-permute-start(bf16[128]{0:T(256)(128)(2,1)S(1)} %get-tuple-element.11), channel_id=1, source_target_pairs={{0,8},{8,16},{16,24},{24,32},{32,40},{40,48},{48,56},{56,64},{64,7... | collective-permute-start | bytes 776 | tf_op jit(solution)/shard_map/ppermute | solution.py:28
  12.9 17.8 %collective-permute-start.3 = (bf16[128]{0:T(256)(128)(2,1)S(1)}, bf16[128]{0:T(256)(128)(2,1)S(1)}, u32[]{:S(2)}, u32[]{:S(2)}) collective-permute-start(bf16[128]{0:T(256)(128)(2,1)S(1)} %get-tuple-element.12), channel_id=1, source_target_pairs={{8,0},{16,8},{24,16},{32,24},{40,32},{48,40},{56,48},{64,56},{72,6... | collective-permute-start | bytes 776 | tf_op jit(solution)/shard_map/ppermute | solution.py:29
  16.0 15.7 %collective-permute-start.4 = (bf16[128,1,64]{0,2,1:T(8,128)(2,1)S(1)}, bf16[128,1,64]{0,2,1:T(8,128)(2,1)S(1)}, u32[]{:S(2)}, u32[]{:S(2)}) collective-permute-start(bf16[128,1,64]{0,2,1:T(8,128)(2,1)S(1)} %get-tuple-element.9), channel_id=1, source_target_pairs={{0,8},{8,16},{16,24},{24,32},{32,40},{40,48},{48,56},{56,64},{64,7... | collective-permute-start | bytes 49160 | tf_op jit(solution)/shard_map/ppermute | solution.py:28
  20.0 11.8 %collective-permute-start.5 = (bf16[128,1,64]{0,2,1:T(8,128)(2,1)S(1)}, bf16[128,1,64]{0,2,1:T(8,128)(2,1)S(1)}, u32[]{:S(2)}, u32[]{:S(2)}) collective-permute-start(bf16[128,1,64]{0,2,1:T(8,128)(2,1)S(1)} %get-tuple-element.10), channel_id=1, source_target_pairs={{8,0},{16,8},{24,16},{32,24},{40,32},{48,40},{56,48},{64,56},{72,6... | collective-permute-start | bytes 49160 | tf_op jit(solution)/shard_map/ppermute | solution.py:29
  22.1 13.7 %collective-permute-start = (bf16[128,1,64]{0,2,1:T(8,128)(2,1)S(1)}, bf16[128,1,64]{0,2,1:T(8,128)(2,1)S(1)}, u32[]{:S(2)}, u32[]{:S(2)}) collective-permute-start(bf16[128,1,64]{0,2,1:T(8,128)(2,1)S(1)} %get-tuple-element.7), channel_id=1, source_target_pairs={{0,8},{8,16},{16,24},{24,32},{32,40},{40,48},{48,56},{56,64},{64,7... | collective-permute-start | bytes 49160 | tf_op jit(solution)/shard_map/ppermute | solution.py:28
  29.4 6.3 %collective-permute-start.1 = (bf16[128,1,64]{0,2,1:T(8,128)(2,1)S(1)}, bf16[128,1,64]{0,2,1:T(8,128)(2,1)S(1)}, u32[]{:S(2)}, u32[]{:S(2)}) collective-permute-start(bf16[128,1,64]{0,2,1:T(8,128)(2,1)S(1)} %get-tuple-element.8), channel_id=1, source_target_pairs={{8,0},{16,8},{24,16},{32,24},{40,32},{48,40},{56,48},{64,56},{72,6... | collective-permute-start | bytes 49160 | tf_op jit(solution)/shard_map/ppermute | solution.py:29
  31.8 1.9 copy-start.3
  33.7 2.1 %copy-start.1 = (bf16[512,64]{0,1:T(8,128)(2,1)S(1)}, bf16[512,64]{0,1:T(8,128)(2,1)}, u32[]{:S(2)}) copy-start(bf16[512,64]{0,1:T(8,128)(2,1)} %param.15) | copy-start | bytes 196612
  40.2 36.6 %copy-start.2 = (f32[2048]{0:T(1024)S(1)}, f32[2048]{0:T(1024)}, u32[]{:S(2)}) copy-start(f32[2048]{0:T(1024)} %param.21) | copy-start | bytes 24580
  40.2 35.1 %all-to-all-start = ((bf16[8,64,2048]{2,1,0:T(8,128)(2,1)}), bf16[8,64,2048]{2,1,0:T(8,128)(2,1)S(1)}, u32[]{:S(2)}, u32[]{:S(2)}) async-start(bf16[8,64,2048]{2,1,0:T(8,128)(2,1)} %bitcast.23), calls=%async_computation | async-start | bytes 4194304 | tf_op jit(solution)/shard_map/all_to_all | solution.py:42
Sparse Core Ops, SparseCore 0:
  10.4 104.5 all-gather.1
where the time goes:
time: 195 us; the launch traced here: 194 us
  blocking collectives  90.6 us (46%)
  waiting for transfers between devices  34.4 us (18%)
  starting transfers between devices  24.7 us (13%)
  matrix products  15.6 us (8%)
  between operations  13.7 us (7%)
  other arithmetic  10.7 us (5%)
  local copies, waits for them, and re-layouts  4.41 us (2%)
    all_to_all x2, blocking collectives, copy_for_each(): return lax.all_to_all(copies, axis, split_axis=0, concat_axis=0, tiled=True)  59.3 us
    all_to_all x1, blocking collectives, summed_on_arrival(): tiles = lax.all_to_all(in_blocks(x, dim, count), axis, 0, 0, tiled=True)  31.3 us
    all_to_all x1, waiting for transfers between devices, summed_on_arrival(): tiles = lax.all_to_all(in_blocks(x, dim, count), axis, 0, 0, tiled=True)  26.2 us
    ppermute x3, starting transfers between devices, extended(): before = lax.ppermute(last, axis, up)  12 us
    dot_general x1, matrix products, mixer_partial(): return jnp.dot(active, gathered[1], preferred_element_type=jnp.float32)  9.31 us
    all_to_all x1, starting transfers between devices, summed_on_arrival(): tiles = lax.all_to_all(in_blocks(x, dim, count), axis, 0, 0, tiled=True)  8.88 us
    all_gather x1, waiting for transfers between devices, gather_turned(): result, at, outs = (lax.all_gather(both, axis, axis=0, tiled=True), 0, [])  8.14 us
  transfers between devices with their start and end apart: 8, of which 2 were waited for; matrix products, arithmetic and copies ran while one was open for 9% of the time, Pallas kernels for 0%

commit v1 on v0

--- a/solution.py
+++ b/solution.py
@@ -10,7 +10,13 @@
 def gather_turned(arrays, axis, dims):
     turned = [jnp.moveaxis(a, dim, 0) for a, dim in zip(arrays, dims)]
     both = jnp.concatenate([t.reshape(len(t), -1) for t in turned], axis=1)
-    result, at, outs = (lax.all_gather(both, axis, axis=0, tiled=True), 0, [])
+    result, at, outs = (
+        jnp.concatenate(
+            lax.all_to_all(jnp.stack([both] * lax.axis_size(axis)), axis, 0, 0), axis=0
+        ),
+        0,
+        [],
+    )
     for t, dim in zip(turned, dims):
         section = result[:, at : at + t[0].size].reshape(-1, *t.shape[1:])
         outs.append(jnp.moveaxis(section, 0, dim))

time: 195 us -> 394 us (2.02)
  the two profiles are of different devices: /device:TPU:1 before, /device:TPU:32 now
where the time goes in v1:
time: 394 us; the launch traced here: 393 us
  blocking collectives  281 us (71%)
  waiting for transfers between devices  53.4 us (14%)
  starting transfers between devices  26.4 us (7%)
  matrix products  15.6 us (4%)
  other arithmetic  10 us (3%)
  local copies, waits for them, and re-layouts  6.8 us (2%)
    all_to_all x1, blocking collectives, gather_turned(): lax.all_to_all(jnp.stack([both] * lax.axis_size(axis)), axis, 0, 0)  212 us
    all_to_all x1, blocking collectives, summed_on_arrival(): tiles = lax.all_to_all(in_blocks(x, dim, count), axis, 0, 0, tiled=True)  39.6 us
    all_to_all x1, blocking collectives, copy_for_each(): return lax.all_to_all(copies, axis, split_axis=0, concat_axis=0, tiled=True)  29.7 us
    all_to_all x1, waiting for transfers between devices, summed_on_arrival(): tiles = lax.all_to_all(in_blocks(x, dim, count), axis, 0, 0, tiled=True)  27.2 us
    all_to_all x1, waiting for transfers between devices, copy_for_each(): return lax.all_to_all(copies, axis, split_axis=0, concat_axis=0, tiled=True)  26.2 us
    ppermute x3, starting transfers between devices, extended(): after = lax.ppermute(initial, axis, down)  10.7 us
    dot_general x1, matrix products, mixer_partial(): return jnp.dot(active, gathered[1], preferred_element_type=jnp.float32)  9.28 us
  transfers between devices with their start and end apart: 8, of which 2 were waited for; matrix products, arithmetic and copies ran while one was open for 3% of the time, Pallas kernels for 0%

profile of v1, /device:TPU:32, one launch (start us, length us, event | category | flops | bytes accessed | tf_op | source)
XLA Modules:
  0.0 393.5 jit_solution(11134831291357981238)
XLA Ops:
  0.0 0.8 convert_element_type.85
  0.8 2.3 collective-permute-start.3
  3.1 3.5 collective-permute-start.2
  6.6 0.9 fusion.39
  7.5 0.9 fusion.41
  8.5 3.6 collective-permute-start.5
  12.0 2.3 collective-permute-start.4
  14.3 0.7 slice_bitcast_fusion.3
  15.1 4.8 %collective-permute-start.1 = (bf16[128,1,64]{0,2,1:T(8,128)(2,1)S(1)}, bf16[128,1,64]{0,2,1:T(8,128)(2,1)S(1)}, u32[]{:S(2)}, u32[]{:S(2)}) collective-permute-start(bf16[128,1,64]{0,2,1:T(8,128)(2,1)S(1)} %get-tuple-element.8), channel_id=1, source_target_pairs={{8,0},{16,8},{24,16},{32,24},{40,32},{48,40},{56,48},{64,56},{72,6... | collective-permute-start | bytes 49160 | tf_op jit(solution)/shard_map/ppermute | solution.py:35
  19.9 0.9 fusion.67
  20.8 1.1 copy.15
  21.9 0.1 bitcast_reduce_fusion
  22.0 0.3 fusion.16
  22.4 0.7 mul.141
  23.0 0.1 mul.142
  23.1 0.1 fusion.34
  23.2 1.9 collective-permute-start
  25.2 0.0 collective-permute-done.2
  25.2 1.0 fusion.20
  26.2 0.0 collective-permute-done.5
  26.2 0.0 copy-start.3
  26.2 1.9 fusion.7
  28.1 0.0 copy-start.1
  28.1 0.1 broadcast_maximum_fusion
  28.2 1.9 fusion.1
  30.1 0.1 fusion.54
  30.1 0.0 collective-permute-done.1
  30.1 0.0 collective-permute-done
  30.2 2.3 fusion.30
  32.5 2.1 convolution_convert_fusion
  34.6 4.4 %all-to-all-start = ((bf16[8,64,2048]{2,1,0:T(8,128)(2,1)}), bf16[8,64,2048]{2,1,0:T(8,128)(2,1)S(1)}, u32[]{:S(2)}, u32[]{:S(2)}) async-start(bf16[8,64,2048]{2,1,0:T(8,128)(2,1)} %bitcast.23), calls=%async_computation | async-start | bytes 4194304 | tf_op jit(solution)/shard_map/all_to_all | solution.py:48
  39.0 27.2 %all-to-all-done = bf16[8,64,2048]{2,1,0:T(8,128)(2,1)S(1)} async-done(((bf16[8,64,2048]{2,1,0:T(8,128)(2,1)}), bf16[8,64,2048]{2,1,0:T(8,128)(2,1)S(1)}, u32[]{:S(2)}, u32[]{:S(2)}) %all-to-all-start) | async-done | bytes 2097184 | tf_op jit(solution)/shard_map/all_to_all | solution.py:48
  66.2 0.3 convert_reduce_fusion.1
  66.6 1.1 fusion.35
  67.7 0.1 fusion.37
  67.9 1.6 broadcast_in_dim.14
  69.4 3.6 all-to-all-start.1
  73.1 0.9 pad_maximum_fusion
  73.9 26.2 %all-to-all-done.1 = bf16[8,64,2048]{2,1,0:T(8,128)(2,1)S(1)} async-done(((bf16[8,64,2048]{2,1,0:T(8,128)(2,1)}), bf16[8,64,2048]{2,1,0:T(8,128)(2,1)S(1)}, u32[]{:S(2)}, u32[]{:S(2)}) %all-to-all-start.1) | async-done | bytes 2097184 | tf_op jit(solution)/shard_map/all_to_all | solution.py:60
  100.1 1.1 stack.2
  101.2 211.7 %all_to_all.25 = bf16[64,32,2048]{2,1,0:T(8,128)(2,1)} all-to-all(bf16[64,32,2048]{2,1,0:T(8,128)(2,1)S(1)} %stack.2), channel_id=1, replica_groups=mesh['sp'=64,'tp'=8] {'sp'}, dimensions={0} | all-to-all | bytes 16777216 | tf_op jit(solution)/shard_map/all_to_all | solution.py:15
  312.9 9.3 %fusion.11 = bf16[512,2048]{1,0:T(8,128)(2,1)} fusion(bf16[2048,2048]{1,0:T(8,128)(2,1)} %bitcast.91, bf16[512,2048]{1,0:T(8,128)(2,1)S(1)} %bitcast.93), kind=kOutput, calls=%fused_computation.14 | convolution fusion | flops 4297588736 | bytes 12582912 | tf_op jit(solution)/shard_map/dot_general | solution.py:75
  322.2 39.6 %all_to_all.26 = bf16[8,64,2048]{2,1,0:T(8,128)(2,1)S(1)} all-to-all(bf16[8,64,2048]{2,1,0:T(8,128)(2,1)} %bitcast.94), channel_id=1, replica_groups=mesh['sp'=64,'tp'=8] {'tp'}, dimensions={0} | all-to-all | bytes 4194304 | tf_op jit(solution)/shard_map/all_to_all | solution.py:48
  361.8 0.4 convert_reduce_fusion
  362.2 0.1 fusion.38
  362.2 0.2 broadcast_in_dim.15
  362.5 29.7 %all_to_all.27 = bf16[8,64,2048]{2,1,0:T(8,128)(2,1)S(1)} all-to-all(bf16[8,64,2048]{2,1,0:T(8,128)(2,1)S(1)} %broadcast_in_dim.15), channel_id=1, replica_groups=mesh['sp'=64,'tp'=8] {'tp'}, dimensions={0} | all-to-all | bytes 4194304 | tf_op jit(solution)/shard_map/all_to_all | solution.py:60
  392.1 1.3 copy.19
  (18 shorter events, 0.1 us)
Async XLA Ops:
  0.0 32.5 %copy-start = (bf16[256,2048]{1,0:T(8,128)(2,1)S(1)}, bf16[256,2048]{1,0:T(8,128)(2,1)}, u32[]{:S(2)}) copy-start(bf16[256,2048]{1,0:T(8,128)(2,1)} %param.20) | copy-start | bytes 3145732
  0.8 22.4 %collective-permute-start.3 = (bf16[128]{0:T(256)(128)(2,1)S(1)}, bf16[128]{0:T(256)(128)(2,1)S(1)}, u32[]{:S(2)}, u32[]{:S(2)}) collective-permute-start(bf16[128]{0:T(256)(128)(2,1)S(1)} %get-tuple-element.12), channel_id=1, source_target_pairs={{8,0},{16,8},{24,16},{32,24},{40,32},{48,40},{56,48},{64,56},{72,6... | collective-permute-start | bytes 776 | tf_op jit(solution)/shard_map/ppermute | solution.py:35
  3.1 22.0 %collective-permute-start.2 = (bf16[128]{0:T(256)(128)(2,1)S(1)}, bf16[128]{0:T(256)(128)(2,1)S(1)}, u32[]{:S(2)}, u32[]{:S(2)}) collective-permute-start(bf16[128]{0:T(256)(128)(2,1)S(1)} %get-tuple-element.11), channel_id=1, source_target_pairs={{0,8},{8,16},{16,24},{24,32},{32,40},{40,48},{48,56},{56,64},{64,7... | collective-permute-start | bytes 776 | tf_op jit(solution)/shard_map/ppermute | solution.py:34
  8.5 17.7 %collective-permute-start.5 = (bf16[128,1,64]{0,2,1:T(8,128)(2,1)S(1)}, bf16[128,1,64]{0,2,1:T(8,128)(2,1)S(1)}, u32[]{:S(2)}, u32[]{:S(2)}) collective-permute-start(bf16[128,1,64]{0,2,1:T(8,128)(2,1)S(1)} %get-tuple-element.10), channel_id=1, source_target_pairs={{8,0},{16,8},{24,16},{32,24},{40,32},{48,40},{56,48},{64,56},{72,6... | collective-permute-start | bytes 49160 | tf_op jit(solution)/shard_map/ppermute | solution.py:35
  12.0 14.2 %collective-permute-start.4 = (bf16[128,1,64]{0,2,1:T(8,128)(2,1)S(1)}, bf16[128,1,64]{0,2,1:T(8,128)(2,1)S(1)}, u32[]{:S(2)}, u32[]{:S(2)}) collective-permute-start(bf16[128,1,64]{0,2,1:T(8,128)(2,1)S(1)} %get-tuple-element.9), channel_id=1, source_target_pairs={{0,8},{8,16},{16,24},{24,32},{32,40},{40,48},{48,56},{56,64},{64,7... | collective-permute-start | bytes 49160 | tf_op jit(solution)/shard_map/ppermute | solution.py:34
  15.1 15.1 %collective-permute-start.1 = (bf16[128,1,64]{0,2,1:T(8,128)(2,1)S(1)}, bf16[128,1,64]{0,2,1:T(8,128)(2,1)S(1)}, u32[]{:S(2)}, u32[]{:S(2)}) collective-permute-start(bf16[128,1,64]{0,2,1:T(8,128)(2,1)S(1)} %get-tuple-element.8), channel_id=1, source_target_pairs={{8,0},{16,8},{24,16},{32,24},{40,32},{48,40},{56,48},{64,56},{72,6... | collective-permute-start | bytes 49160 | tf_op jit(solution)/shard_map/ppermute | solution.py:35
  23.2 6.9 %collective-permute-start = (bf16[128,1,64]{0,2,1:T(8,128)(2,1)S(1)}, bf16[128,1,64]{0,2,1:T(8,128)(2,1)S(1)}, u32[]{:S(2)}, u32[]{:S(2)}) collective-permute-start(bf16[128,1,64]{0,2,1:T(8,128)(2,1)S(1)} %get-tuple-element.7), channel_id=1, source_target_pairs={{0,8},{8,16},{16,24},{24,32},{32,40},{40,48},{48,56},{56,64},{64,7... | collective-permute-start | bytes 49160 | tf_op jit(solution)/shard_map/ppermute | solution.py:34
  26.2 1.9 copy-start.3
  28.1 2.1 copy-start.1
  34.6 33.1 %copy-start.2 = (f32[2048]{0:T(1024)S(1)}, f32[2048]{0:T(1024)}, u32[]{:S(2)}) copy-start(f32[2048]{0:T(1024)} %param.21) | copy-start | bytes 24580
  34.6 31.6 %all-to-all-start = ((bf16[8,64,2048]{2,1,0:T(8,128)(2,1)}), bf16[8,64,2048]{2,1,0:T(8,128)(2,1)S(1)}, u32[]{:S(2)}, u32[]{:S(2)}) async-start(bf16[8,64,2048]{2,1,0:T(8,128)(2,1)} %bitcast.23), calls=%async_computation | async-start | bytes 4194304 | tf_op jit(solution)/shard_map/all_to_all | solution.py:48
  69.4 30.7 %all-to-all-start.1 = ((bf16[8,64,2048]{2,1,0:T(8,128)(2,1)}), bf16[8,64,2048]{2,1,0:T(8,128)(2,1)S(1)}, u32[]{:S(2)}, u32[]{:S(2)}) async-start(bf16[8,64,2048]{2,1,0:T(8,128)(2,1)} %broadcast_in_dim.14), calls=%async_computation.1 | async-start | bytes 4194304 | tf_op jit(solution)/shard_map/all_to_all | solution.py:60
